TPU v7x, 256 devices: a whole 4x4x8 slice. The times are simulated.
256 devices in a mesh: fs: 32 (over z, y), tp: 8 (over x, core).
Axes of the slice: x: 4, y: 4, z: 8, core: 2. Of those that a mesh axis runs over, the one named last changes fastest.
Arguments:
- prompt: bfloat16 [32768, 2048], P(('fs', 'tp')), may hold values from -6 to 6
- norm_gain: float32 [2048], P('fs'), may hold values from 0.1 to 1.9
- up_trained: float32 [2048, 8192], P('fs', 'tp'), may hold values from -0.125 to 0.125
- down_trained: float32 [2048, 8192], P('fs', 'tp'), may hold values from -0.0625 to 0.0625
Outputs:
- up_served: bfloat16 [2048, 8192], P(None, 'tp')
- down_served: bfloat16 [8192, 2048], P('tp')
- mixed: bfloat16 [32768, 2048], P(('fs', 'tp'))
All inputs are finite; a program needn't handle non-finite values.
Results may differ from a plain program's by a relative error of at most 0.014.
Values may be sent and summed in bfloat16 or wider, within the bound.
No kernel may reach another device: no remote copies, remote signals or barrier semaphores. Data moves between devices by JAX's collectives and lax.ppermute only.
A program may use at most 128 MiB of HBM per device.

v0:
```python
import jax
import jax.numpy as jnp
from jax import lax
from jax.sharding import PartitionSpec as P


def sent_together(arrays, axis, dim, along):
    both = jnp.concatenate(arrays, axis=along)
    filled, at, finished = (lax.all_gather(both, axis, axis=dim, tiled=True), 0, [])
    for a in arrays:
        finished.append(lax.slice_in_dim(filled, at, at + a.shape[along], axis=along))
        at += a.shape[along]
    return tuple(finished)


def shards(prompt, norm_gain, up_trained, down_trained):
    up_local = (norm_gain[:, None] * up_trained).astype(jnp.bfloat16)
    down_local = down_trained.astype(jnp.bfloat16)
    values = prompt.astype(jnp.float32)
    scale = lax.rsqrt(jnp.mean(values * values, axis=-1, keepdims=True) + 1e-06)
    normed = (values * scale).astype(jnp.bfloat16)
    group_rows = lax.all_gather(normed, "tp", axis=0, tiled=True)
    up_whole, down_whole = sent_together((up_local, down_local), "fs", 0, 1)
    pre = jnp.dot(group_rows, up_whole, preferred_element_type=jnp.float32)
    hidden = jnp.square(jax.nn.relu(pre)).astype(jnp.bfloat16)
    down_served = jnp.transpose(down_whole)
    mixed = lax.psum_scatter(
        jnp.dot(hidden, down_served, preferred_element_type=jnp.float32).astype(jnp.bfloat16),
        "tp",
        scatter_dimension=0,
        tiled=True,
    )
    return (up_whole, down_served, mixed)


def solution(mesh):
    return jax.shard_map(
        shards,
        mesh=mesh,
        in_specs=(P(("fs", "tp"), None), P("fs"), P("fs", "tp"), P("fs", "tp")),
        out_specs=(P(None, "tp"), P("tp", None), P(("fs", "tp"), None)),
        check_vma=False,
    )
```

profile of v0, /device:TPU:8, one launch (start us, length us, event | category | flops | bytes accessed | tf_op | source)
XLA Modules:
  0.0 207.6 jit_solution(5565873400041753207)
XLA Ops:
  7.2 0.0 all-gather.3.cloned.1.call-start
  7.2 1.0 convert_element_type.19
  8.2 1.0 multiply_convert_fusion.1
  9.2 0.7 pad_maximum_fusion
  9.9 0.0 all-gather.3.cloned.1.call-update
  10.0 0.0 all-gather.5.cloned.1.call-start
  10.0 1.2 fusion.1
  11.3 2.0 fusion.2
  13.2 0.0 all-gather.5.cloned.1.call-update
  13.3 0.0 reduce-scatter.2.cloned.1.call-start
  13.3 97.3 %all-gather.3.cloned.1.call-done = bf16[2048,2048]{1,0:T(8,128)(2,1)} async-done(((bf16[64,2048]{1,0:T(8,128)(2,1)}), bf16[2048,2048]{1,0:T(8,128)(2,1)}) %all-gather.3.cloned.1.call-update) | async-done | bytes 8388624 | tf_op jit(solution)/shard_map/all_gather | solution.py:9
  110.7 6.0 %slice_bitcast_fusion = (bf16[1024,2048]{0,1:T(8,128)(2,1)}, bf16[2048,1024]{1,0:T(8,128)(2,1)}) fusion(bf16[2048,2048]{1,0:T(8,128)(2,1)} %all-gather.3.cloned.1.call-done), kind=kLoop, calls=%fused_computation.3 | loop fusion | bytes 16777216 | tf_op jit(solution)/shard_map/transpose | solution.py:26
  116.7 29.4 %all-gather.5.cloned.1.call-done = bf16[1024,2048]{1,0:T(8,128)(2,1)} async-done(((bf16[128,2048]{1,0:T(8,128)(2,1)}), bf16[1024,2048]{1,0:T(8,128)(2,1)}) %all-gather.5.cloned.1.call-update) | async-done | bytes 4194320 | tf_op jit(solution)/shard_map/all_gather | solution.py:22
  146.0 14.4 %convolution_convert_fusion = bf16[1024,2048]{1,0:T(8,128)(2,1)} fusion(bf16[2048,2048]{1,0:T(8,128)(2,1)} %all-gather.3.cloned.1.call-done, bf16[1024,2048]{1,0:T(8,128)(2,1)} %all-gather.5.cloned.1.call-done, bf16[2048,1024]{1,0:T(8,128)(2,1)} %get-tuple-element.10), kind=kOutput, calls=%fused_computation.1 | convolution fusion | flops 8595177472 | bytes 16777216 | tf_op jit(solution)/shard_map/dot_general | solution.py:28
  160.4 0.0 reduce-scatter.2.cloned.1.call-update
  160.4 6.4 %copy.10 = bf16[1024,2048]{1,0:T(8,128)(2,1)} copy(bf16[1024,2048]{0,1:T(8,128)(2,1)} %get-tuple-element.9) | data formatting | bytes 8388608
  166.9 34.2 %reduce-scatter.2.cloned.1.call-done = bf16[128,2048]{1,0:T(8,128)(2,1)} async-done(((bf16[1024,2048]{1,0:T(8,128)(2,1)}), bf16[128,2048]{1,0:T(8,128)(2,1)}) %reduce-scatter.2.cloned.1.call-update) | async-done | bytes 524304 | tf_op jit(solution)/shard_map/reduce_scatter | solution.py:27
  (1 shorter events, 0.0 us)
Async XLA Ops:
  7.2 103.5 %all-gather.3.cloned.1.call-start = ((), (), s32[]{:S(2)}) async-start(), calls=%async_computation.1 | async-start | bytes 8650752 | tf_op jit(solution)/shard_map/all_gather | solution.py:9
  10.0 136.1 %all-gather.5.cloned.1.call-start = ((), (), s32[]{:S(2)}) async-start(), calls=%async_computation.2 | async-start | bytes 4718592 | tf_op jit(solution)/shard_map/all_gather | solution.py:22
  13.3 187.8 %reduce-scatter.2.cloned.1.call-start = ((), (), s32[]{:S(2)}) async-start(), calls=%async_computation.3 | async-start | bytes 4718592 | tf_op jit(solution)/shard_map/reduce_scatter | solution.py:27
Sparse Core Ops, SparseCore 0:
  11.1 99.4 all-gather.2
  113.1 32.8 all-gather.4
  160.5 40.4 reduce-scatter.1
where the time goes:
time: 208 us
  waiting for transfers between devices  161 us (77%)
  matrix products  14.4 us (7%)
  between operations  13.8 us (7%)
  local copies, waits for them, and re-layouts  12.5 us (6%)
  other arithmetic  5.96 us (3%)
    all_gather x1, waiting for transfers between devices, sent_together(): lax.all_gather(both, axis, axis=dim, tiled=True)  97.3 us
    reduce_scatter x1, waiting for transfers between devices, shards(): lax.psum_scatter(jnp.dot(hidden, down_served, preferred_element_type=jnp....  34.2 us
    all_gather x1, waiting for transfers between devices, shards(): group_rows = lax.all_gather(normed, 'tp', axis=0, tiled=True)  29.4 us
    dot_general x1, matrix products, shards(): jnp.dot(hidden, down_served, preferred_element_type=jnp.float32)  14.4 us
    unnamed x1, local copies, waits for them, and re-layouts  6.43 us
    transpose x1, local copies, waits for them, and re-layouts, shards(): down_served = jnp.transpose(down_whole)  6.02 us
  transfers between devices with their start and end apart: 3, of which 3 were waited for; matrix products, arithmetic and copies ran while one was open for 8% of the time, Pallas kernels for 0%

commit v1 on v0

--- a/solution.py
+++ b/solution.py
@@ -2,6 +2,11 @@
 import jax.numpy as jnp
 from jax import lax
 from jax.sharding import PartitionSpec as P
+
+
+def gather_by_exchange(array, axis, dim):
+    copies = jnp.concatenate([array] * lax.axis_size(axis), axis=dim)
+    return lax.all_to_all(copies, axis, dim, dim, tiled=True)
 
 
 def sent_together(arrays, axis, dim, along):
@@ -19,7 +24,7 @@
     values = prompt.astype(jnp.float32)
     scale = lax.rsqrt(jnp.mean(values * values, axis=-1, keepdims=True) + 1e-06)
     normed = (values * scale).astype(jnp.bfloat16)
-    group_rows = lax.all_gather(normed, "tp", axis=0, tiled=True)
+    group_rows = gather_by_exchange(normed, "tp", 0)
     up_whole, down_whole = sent_together((up_local, down_local), "fs", 0, 1)
     pre = jnp.dot(group_rows, up_whole, preferred_element_type=jnp.float32)
     hidden = jnp.square(jax.nn.relu(pre)).astype(jnp.bfloat16)

time: 208 us -> 177 us (0.85)
  waiting for transfers between devices: 161 us -> 122 us
  starting transfers between devices: 0.12 us -> 4.67 us
    all_gather x1 -> x0, waiting for transfers between devices: 29.4 us -> none  [shards(): group_rows = lax.all_gather(normed, 'tp', axis=0, tiled=True)]
    all_gather x1, waiting for transfers between devices: 97.3 us -> 89.5 us  [sent_together(): lax.all_gather(both, axis, axis=dim, tiled=True)]
    all_to_all x0 -> x1, starting transfers between devices: none -> 4.59 us  [gather_by_exchange(): return lax.all_to_all(copies, axis, dim, dim, tiled=True)]
    unnamed x0 -> x7, other arithmetic: none -> 3.18 us
    unnamed x1 -> x5, local copies, waits for them, and re-layouts: 6.43 us -> 8.45 us
  transfers between devices with their start and end apart: 3 -> 3, of which waited for: 3 -> 2; matrix products, arithmetic and copies ran while one was open for 8% -> 10% of each run, Pallas kernels for 0% -> 0%
where the time goes in v1:
time: 177 us
  waiting for transfers between devices  122 us (69%)
  local copies, waits for them, and re-layouts  14.5 us (8%)
  matrix products  14.4 us (8%)
  between operations  14.1 us (8%)
  other arithmetic  7.35 us (4%)
  starting transfers between devices  4.67 us (3%)
    all_gather x1, waiting for transfers between devices, sent_together(): lax.all_gather(both, axis, axis=dim, tiled=True)  89.5 us
    reduce_scatter x1, waiting for transfers between devices, shards(): lax.psum_scatter(jnp.dot(hidden, down_served, preferred_element_type=jnp....  32.5 us
    dot_general x1, matrix products, shards(): jnp.dot(hidden, down_served, preferred_element_type=jnp.float32)  14.4 us
    unnamed x5, local copies, waits for them, and re-layouts  8.45 us
    transpose x1, local copies, waits for them, and re-layouts, shards(): down_served = jnp.transpose(down_whole)  6.02 us
    all_to_all x1, starting transfers between devices, gather_by_exchange(): return lax.all_to_all(copies, axis, dim, dim, tiled=True)  4.59 us
  transfers between devices with their start and end apart: 3, of which 2 were waited for; matrix products, arithmetic and copies ran while one was open for 10% of the time, Pallas kernels for 0%

profile of v1, /device:TPU:8, one launch (start us, length us, event | category | flops | bytes accessed | tf_op | source)
XLA Modules:
  0.0 176.9 jit_solution(13976503917289991912)
XLA Ops:
  7.2 0.0 copy-start
  7.2 0.0 all-gather.2.cloned.1.call-start
  7.2 1.0 convert_element_type.19
  8.2 1.0 multiply_convert_fusion.1
  9.3 0.7 pad_maximum_fusion
  10.0 0.0 all-gather.2.cloned.1.call-update
  10.0 1.2 fusion.1
  11.3 1.2 constant_dynamic-update-slice_fusion.7
  12.5 1.2 constant_dynamic-update-slice_fusion.6
  13.7 0.0 copy-done
  13.7 0.2 constant_dynamic-update-slice_fusion.5
  13.8 0.2 constant_dynamic-update-slice_fusion.4
  14.0 0.2 constant_dynamic-update-slice_fusion.3
  14.2 0.2 constant_dynamic-update-slice_fusion.2
  14.3 0.2 constant_dynamic-update-slice_fusion.1
  14.5 0.2 constant_dynamic-update-slice_fusion
  14.6 0.0 copy-start.1
  14.6 2.0 %copy-done.1 = bf16[1024,2048]{1,0:T(8,128)(2,1)} copy-done((bf16[1024,2048]{1,0:T(8,128)(2,1)}, bf16[1024,2048]{1,0:T(8,128)(2,1)S(1)}, u32[]{:S(2)}) %copy-start.1) | copy-done | bytes 4194328
  16.7 4.6 %all-to-all-start = ((bf16[8,128,2048]{2,1,0:T(8,128)(2,1)}), bf16[8,128,2048]{2,1,0:T(8,128)(2,1)}, u32[]{:S(2)}, u32[]{:S(2)}) async-start(bf16[8,128,2048]{2,1,0:T(8,128)(2,1)} %bitcast.6), calls=%async_computation | async-start | bytes 8388608 | tf_op jit(solution)/shard_map/all_to_all | solution.py:9
  21.3 0.0 reduce-scatter.2.cloned.1.call-start
  21.3 89.5 %all-gather.2.cloned.1.call-done = bf16[2048,2048]{1,0:T(8,128)(2,1)} async-done(((bf16[64,2048]{1,0:T(8,128)(2,1)}), bf16[2048,2048]{1,0:T(8,128)(2,1)}) %all-gather.2.cloned.1.call-update) | async-done | bytes 8388624 | tf_op jit(solution)/shard_map/all_gather | solution.py:14
  110.8 6.0 %slice_bitcast_fusion = (bf16[1024,2048]{0,1:T(8,128)(2,1)}, bf16[2048,1024]{1,0:T(8,128)(2,1)}) fusion(bf16[2048,2048]{1,0:T(8,128)(2,1)} %all-gather.2.cloned.1.call-done), kind=kLoop, calls=%fused_computation.3 | loop fusion | bytes 16777216 | tf_op jit(solution)/shard_map/transpose | solution.py:31
  116.8 0.0 all-to-all-done
  116.8 14.4 %convolution_convert_fusion = bf16[1024,2048]{1,0:T(8,128)(2,1)} fusion(bf16[2048,2048]{1,0:T(8,128)(2,1)} %all-gather.2.cloned.1.call-done, bf16[1024,2048]{1,0:T(8,128)(2,1)} %bitcast.2, bf16[2048,1024]{1,0:T(8,128)(2,1)} %get-tuple-element.10), kind=kOutput, calls=%fused_computation.1 | convolution fusion | flops 8595177472 | bytes 16777216 | tf_op jit(solution)/shard_map/dot_general | solution.py:33
  131.2 0.0 reduce-scatter.2.cloned.1.call-update
  131.2 6.4 %copy.10 = bf16[1024,2048]{1,0:T(8,128)(2,1)} copy(bf16[1024,2048]{0,1:T(8,128)(2,1)} %get-tuple-element.9) | data formatting | bytes 8388608
  137.6 32.5 %reduce-scatter.2.cloned.1.call-done = bf16[128,2048]{1,0:T(8,128)(2,1)} async-done(((bf16[1024,2048]{1,0:T(8,128)(2,1)}), bf16[128,2048]{1,0:T(8,128)(2,1)}) %reduce-scatter.2.cloned.1.call-update) | async-done | bytes 524304 | tf_op jit(solution)/shard_map/reduce_scatter | solution.py:32
  (1 shorter events, 0.0 us)
Async XLA Ops:
  7.2 6.5 %copy-start = (bf16[128,2048]{1,0:T(8,128)(2,1)S(1)}, bf16[128,2048]{1,0:T(8,128)(2,1)}, u32[]{:S(2)}) copy-start(bf16[128,2048]{1,0:T(8,128)(2,1)} %param.4) | copy-start | bytes 1572868
  7.2 103.6 %all-gather.2.cloned.1.call-start = ((), (), s32[]{:S(2)}) async-start(), calls=%async_computation.2 | async-start | bytes 8650752 | tf_op jit(solution)/shard_map/all_gather | solution.py:14
  14.6 2.0 %copy-start.1 = (bf16[1024,2048]{1,0:T(8,128)(2,1)}, bf16[1024,2048]{1,0:T(8,128)(2,1)S(1)}, u32[]{:S(2)}) copy-start(bf16[1024,2048]{1,0:T(8,128)(2,1)S(1)} %constant_dynamic-update-slice_fusion) | copy-start | bytes 12582916
  16.7 100.2 %all-to-all-start = ((bf16[8,128,2048]{2,1,0:T(8,128)(2,1)}), bf16[8,128,2048]{2,1,0:T(8,128)(2,1)}, u32[]{:S(2)}, u32[]{:S(2)}) async-start(bf16[8,128,2048]{2,1,0:T(8,128)(2,1)} %bitcast.6), calls=%async_computation | async-start | bytes 8388608 | tf_op jit(solution)/shard_map/all_to_all | solution.py:9
  21.3 148.8 %reduce-scatter.2.cloned.1.call-start = ((), (), s32[]{:S(2)}) async-start(), calls=%async_computation.3 | async-start | bytes 4718592 | tf_op jit(solution)/shard_map/reduce_scatter | solution.py:32
Sparse Core Ops, SparseCore 0:
  11.1 99.6 all-gather.1
  131.3 38.7 reduce-scatter.1
